TPU v7x, 512 devices: a whole 4x8x8 slice. The times are simulated.
512 devices in a mesh: tp: 64 (over z, y), dp: 8 (over x, core).
Axes of the slice: x: 4, y: 8, z: 8, core: 2. Of those that a mesh axis runs over, the one named last changes fastest.
Arguments:
- hidden: bfloat16 [64, 4096], P(None, 'dp'), may hold values from -6 to 6
- norm_gain: float32 [2, 4096], P(None, 'dp'), may hold values from 0.1 to 1.9
- gate_weight: bfloat16 [2, 4096, 8192], P(None, 'dp', 'tp'), may hold values from -0.09375 to 0.09375
- inner_weight: bfloat16 [2, 4096, 8192], P(None, 'dp', 'tp'), may hold values from -0.09375 to 0.09375
- write_weight: bfloat16 [2, 4096, 2048], P(None, 'dp', 'tp'), may hold values from -0.09375 to 0.09375
- read_weight: bfloat16 [2, 4096, 2048], P(None, 'dp', 'tp'), may hold values from -0.09375 to 0.09375
- step_weight: bfloat16 [2, 4096, 128], P(None, 'dp'), may hold values from -0.09375 to 0.09375
- conv_inner: bfloat16 [2, 4, 8192], P(None, None, 'tp'), may hold values from -3 to 3
- conv_write: bfloat16 [2, 4, 2048], P(None, None, 'tp'), may hold values from -3 to 3
- conv_read: bfloat16 [2, 4, 2048], P(None, None, 'tp'), may hold values from -3 to 3
- step_bias: float32 [2, 128], P(None, 'tp'), may hold values from -4 to -1
- decay_log: float32 [2, 128], P(None, 'tp'), may hold values from -3 to 0.5
- skip_gain: float32 [2, 128], P(None, 'tp'), may hold values from 0.1 to 1.9
- group_gain: float32 [2, 8192], P(None, 'tp'), may hold values from 0.1 to 1.9
- out_weight: bfloat16 [2, 8192, 4096], P(None, 'tp', 'dp'), may hold values from -0.4 to 0.4
- state_inner: bfloat16 [2, 64, 3, 8192], P(None, 'dp', None, 'tp'), may hold values from -6 to 6
- state_write: bfloat16 [2, 64, 3, 2048], P(None, 'dp', None, 'tp'), may hold values from -6 to 6
- state_read: bfloat16 [2, 64, 3, 2048], P(None, 'dp', None, 'tp'), may hold values from -6 to 6
- recurrent: float32 [2, 64, 128, 64, 128], P(None, 'dp', 'tp'), may hold values from -1.2 to 1.2, as said below
Outputs:
- out_hidden: bfloat16 [64, 4096], P(None, 'dp')
- next_inner: bfloat16 [2, 64, 3, 8192], P(None, 'dp', None, 'tp')
- next_write: bfloat16 [2, 64, 3, 2048], P(None, 'dp', None, 'tp')
- next_read: bfloat16 [2, 64, 3, 2048], P(None, 'dp', None, 'tp')
- next_recurrent: float32 [2, 64, 128, 64, 128], P(None, 'dp', 'tp')
Inputs may be any that keep to these rules, and one draw needn't show every extreme that they name: recurrent states of order a tenth, with scales that differ between heads.
All inputs are finite; a program needn't handle non-finite values.
Results may differ from a plain program's by a relative error of at most 0.025.
Values may be sent and summed in bfloat16 or wider, within the bound.
No kernel may reach another device: no remote copies, remote signals or barrier semaphores. Data moves between devices by JAX's collectives and lax.ppermute only.
A program may use at most 64 MiB of HBM per device.

v0:
```python
import jax
import jax.numpy as jnp
from jax import lax
from jax.sharding import Mesh
from jax.sharding import PartitionSpec as P

D = 4096
HEADS = 128
GROUPS = 16
DP = ("dp_0", "dp_1")
TP = ("tp_0", "tp_1")
TP_DP = ("tp_0", "tp_1", "dp_0", "dp_1")
eps = 1e-06


def cut_along(shard, dim, size):
    before, after = (shard.shape[:dim], shard.shape[dim + 1 :])
    return jnp.moveaxis(shard.reshape(*before, size, -1, *after), dim, 0)


def summed_on_arrival(shard, axis, dim):
    size = lax.axis_size(axis)
    pieces = lax.all_to_all(cut_along(shard, dim, size), axis, 0, 0, tiled=True)
    return jnp.sum(pieces.astype(jnp.float32), axis=0)


def side_by_side(arrays, axis, dim, along):
    widths = [a.shape[along] for a in arrays]
    both = jnp.concatenate(arrays, axis=along)
    result = summed_on_arrival(both, axis, dim)
    return tuple(jnp.split(result, [sum(widths[:k]) for k in range(1, len(widths))], axis=along))


def gather_turned(arrays, axis, dims):
    turned = [jnp.moveaxis(a, dim, 0) for a, dim in zip(arrays, dims)]
    both = jnp.concatenate([t.reshape(len(t), -1) for t in turned], axis=1)
    result, at, gathered = (lax.all_gather(both, axis, axis=0, tiled=True), 0, [])
    for t, dim in zip(turned, dims):
        share = result[:, at : at + t[0].size].reshape(-1, *t.shape[1:])
        gathered.append(jnp.moveaxis(share, 0, dim))
        at += t[0].size
    return tuple(gathered)


def over_axes(shard, axes):
    for axis in axes:
        shard = lax.psum(shard, axis)
    return shard


def copy_for_each(shard, axis):
    size = lax.axis_size(axis)
    return lax.all_to_all(
        jnp.broadcast_to(shard[None], (size, *shard.shape)), axis, 0, 0, tiled=True
    )


def laid_out(pieces, dim):
    lengths = list(pieces.shape[1:])
    lengths[dim] *= pieces.shape[0]
    return jnp.moveaxis(pieces, 0, dim).reshape(lengths)


def collect(shard, axis, dim):
    pieces = copy_for_each(shard, axis)
    return laid_out(pieces, dim)


def summed_on_arrival_2(shard, axis, dim):
    pieces = cut_along(shard, dim, lax.axis_size(axis))
    arrived = lax.all_to_all(pieces, axis, split_axis=0, concat_axis=0, tiled=True)
    return arrived.sum(axis=0)


def taken_together(shard, axis):
    return copy_for_each(shard, axis).sum(axis=0)


def convolve(state, fresh_row, kernel):
    window = jnp.concatenate([state, fresh_row[:, None, :]], axis=1)
    summed = jnp.sum(window.astype(jnp.float32) * kernel.astype(jnp.float32)[None], axis=1)
    return (jax.nn.silu(summed), window[:, 1:])


def mixer_block(normed, number, weights):
    (
        gate_weight,
        inner_weight,
        write_weight,
        read_weight,
        step_weight,
        conv_inner,
        conv_write,
        conv_read,
        step_bias,
        decay_log,
        skip_gain,
        group_gain,
        out_weight,
        state_inner,
        state_write,
        state_read,
        recurrent,
    ) = weights

    def partial_of(weight):
        return jnp.dot(normed, weight[number], preferred_element_type=jnp.float32).astype(
            jnp.bfloat16
        )

    summed = side_by_side(
        (
            partial_of(gate_weight),
            partial_of(inner_weight),
            partial_of(write_weight),
            partial_of(read_weight),
            partial_of(step_weight),
        ),
        DP,
        0,
        1,
    )
    gate_raw, inner_raw, write_raw, read_raw, step_raw = [
        member.astype(jnp.bfloat16) for member in summed
    ]
    inner_act, next_inner = convolve(state_inner[number], inner_raw, conv_inner[number])
    write_act, next_write = convolve(state_write[number], write_raw, conv_write[number])
    read_act, next_read = convolve(state_read[number], read_raw, conv_read[number])
    write_all, read_all = gather_turned(
        (write_act.astype(jnp.bfloat16), read_act.astype(jnp.bfloat16)), TP, (1, 1)
    )
    heads_here = step_bias.shape[1]
    head_dim = recurrent.shape[3]
    state_dim = recurrent.shape[4]
    rows_here = inner_act.shape[0]
    first_head = lax.axis_index(TP) * heads_here
    group_index = first_head // (HEADS // GROUPS)
    write_grid = write_all.reshape(rows_here, state_dim, GROUPS)
    read_grid = read_all.reshape(rows_here, state_dim, GROUPS)
    write_vec = lax.dynamic_slice_in_dim(write_grid, group_index, 1, 2)[:, :, 0].astype(jnp.float32)
    read_vec = lax.dynamic_slice_in_dim(read_grid, group_index, 1, 2)[:, :, 0].astype(jnp.float32)
    step_own = lax.dynamic_slice_in_dim(step_raw, first_head, heads_here, 1)
    step_size = jax.nn.softplus(step_own.astype(jnp.float32) + step_bias[number][None, :])
    retain = jnp.exp(-step_size * jnp.exp(decay_log[number])[None, :])
    inner_heads = inner_act.reshape(rows_here, heads_here, head_dim)
    updated = (
        retain[:, :, None, None] * recurrent[number]
        + (step_size[:, :, None] * inner_heads)[:, :, :, None] * write_vec[:, None, None, :]
    )
    readout = jnp.einsum("bhpn,bn->bhp", updated, read_vec, precision=lax.Precision.HIGHEST)
    readout = readout + skip_gain[number][None, :, None] * inner_heads
    gated_out = readout.reshape(rows_here, heads_here * head_dim) * jax.nn.silu(
        gate_raw.astype(jnp.float32)
    )
    selector = (jnp.arange(GROUPS) == group_index).astype(jnp.float32)
    totals = over_axes(jnp.sum(gated_out * gated_out, axis=1)[:, None] * selector[None, :], TP)
    group_sum = jnp.sum(totals * selector[None, :], axis=1, keepdims=True)
    group_factor = lax.rsqrt(group_sum / (HEADS // GROUPS * head_dim) + eps)
    group_normed = (gated_out * group_factor * group_gain[number][None, :]).astype(jnp.bfloat16)
    branch = jnp.dot(
        collect(group_normed, DP, 0), out_weight[number], preferred_element_type=jnp.float32
    )
    return (branch, (next_inner, next_write, next_read, updated))


def columns_over(branch):
    return summed_on_arrival_2(branch, TP, 1)


def local(
    hidden,
    norm_gain,
    gate_weight,
    inner_weight,
    write_weight,
    read_weight,
    step_weight,
    conv_inner,
    conv_write,
    conv_read,
    step_bias,
    decay_log,
    skip_gain,
    group_gain,
    out_weight,
    state_inner,
    state_write,
    state_read,
    recurrent,
):
    weights = (
        gate_weight,
        inner_weight,
        write_weight,
        read_weight,
        step_weight,
        conv_inner,
        conv_write,
        conv_read,
        step_bias,
        decay_log,
        skip_gain,
        group_gain,
        out_weight,
        state_inner,
        state_write,
        state_read,
        recurrent,
    )
    wide_in = hidden.astype(jnp.float32)
    squares = taken_together(jnp.sum(wide_in * wide_in, axis=1, keepdims=True), DP)
    normed = (wide_in * lax.rsqrt(squares / D + eps) * norm_gain[0][None, :]).astype(jnp.bfloat16)
    branch, first_states = mixer_block(normed, 0, weights)
    slice_width = hidden.shape[1] // lax.axis_size(TP)
    offset = lax.axis_index(TP) * slice_width
    own_cols = lax.dynamic_slice_in_dim(wide_in, offset, slice_width, 1)
    middle = (own_cols + columns_over(branch)).astype(jnp.bfloat16).astype(jnp.float32)
    squares = over_axes(jnp.sum(middle * middle, axis=1, keepdims=True), TP_DP)
    gain_slice = lax.dynamic_slice_in_dim(norm_gain[1], offset, slice_width, 0)
    normed_part = (middle * lax.rsqrt(squares / D + eps) * gain_slice[None, :]).astype(jnp.bfloat16)
    normed = collect(normed_part, TP, 1)
    branch, second_states = mixer_block(normed, 1, weights)
    result = collect((middle + columns_over(branch)).astype(jnp.bfloat16), TP, 1)
    stacked = [jnp.stack([earlier, later]) for earlier, later in zip(first_states, second_states)]
    return (result, stacked[0], stacked[1], stacked[2], stacked[3])


def solution(mesh):
    finer = Mesh(mesh.devices.reshape(8, 8, 4, 2), ("tp_0", "tp_1", "dp_0", "dp_1"))
    placed = (
        P(None, DP),
        P(None, DP),
        P(None, DP, TP),
        P(None, DP, TP),
        P(None, DP, TP),
        P(None, DP, TP),
        P(None, DP, None),
        P(None, None, TP),
        P(None, None, TP),
        P(None, None, TP),
        P(None, TP),
        P(None, TP),
        P(None, TP),
        P(None, TP),
        P(None, TP, DP),
        P(None, DP, None, TP),
        P(None, DP, None, TP),
        P(None, DP, None, TP),
        P(None, DP, TP, None, None),
    )
    return jax.shard_map(
        local,
        mesh=finer,
        in_specs=placed,
        out_specs=(
            P(None, DP),
            P(None, DP, None, TP),
            P(None, DP, None, TP),
            P(None, DP, None, TP),
            P(None, DP, TP, None, None),
        ),
        check_vma=False,
    )
```

profile of v0, /device:TPU:8, one launch (start us, length us, event | category | flops | bytes accessed | tf_op | source)
XLA Modules:
  0.0 351.3 jit_solution(7885808371134442058)
XLA Ops:
  0.6 1.0 copy.87
  1.7 0.6 broadcast_in_dim.24
  2.3 4.4 %all-to-all-start = ((f32[8,64,1]{1,2,0:T(1,128)}), f32[8,64,1]{1,2,0:T(1,128)S(1)}, u32[]{:S(2)}, u32[]{:S(2)}) async-start(f32[8,64,1]{1,2,0:T(1,128)} %broadcast_in_dim.24), calls=%async_computation | async-start | bytes 8192 | tf_op jit(solution)/shard_map/all_to_all | solution.py:53
  6.8 0.7 copy-done.12
  7.5 0.7 copy-done.13
  8.2 0.6 copy-done.8
  8.9 3.0 all-to-all-done
  12.0 0.3 convolution_convert_fusion.8
  12.4 0.4 copy-done.5
  12.8 0.3 convolution_convert_fusion.9
  13.2 0.3 convolution_convert_fusion.4
  13.5 0.5 copy-done.2
  14.0 0.3 convolution_convert_fusion.3
  14.3 0.6 copy-done.4
  14.9 0.3 convolution_convert_fusion.5
  15.3 0.7 concatenate.30
  16.0 3.4 all-to-all-start.1
  19.4 5.5 %all-to-all-done.1 = bf16[8,8,448]{2,1,0:T(8,128)(2,1)S(1)} async-done(((bf16[8,8,448]{2,1,0:T(8,128)(2,1)}), bf16[8,8,448]{2,1,0:T(8,128)(2,1)S(1)}, u32[]{:S(2)}, u32[]{:S(2)}) %all-to-all-start.1) | async-done | bytes 57376 | tf_op jit(solution)/shard_map/all_to_all | solution.py:23
  25.2 56.1 %all-gather = bf16[64,32,16]{1,2,0:T(8,128)(2,1)S(1)} all-gather(bf16[1,32,16]{1,2,0:T(8,128)(2,1)S(1)} %maximum_bitcast_fusion), channel_id=1, replica_groups=mesh['tp_0'=8,'tp_1'=8,'dp_0'=4,'dp_1'=2] {'tp_0','tp_1'}, dimensions={0}, use_global_device_ids=true | all-gather | bytes 66560 | tf_op jit(solution)/shard_map/all_gather | solution.py:37
  81.4 0.3 reshape.168
  82.3 0.3 dynamic-slice_reduce_fusion.1
  82.8 0.8 fusion.4
  84.0 16.0 %psum.56 = f32[8,16]{1,0:T(8,128)S(1)} all-reduce(f32[8,16]{1,0:T(8,128)S(1)} %broadcast_multiply_fusion.3), channel_id=1, replica_groups=mesh['tp_0'=8,'tp_1'=8,'dp_0'=4,'dp_1'=2] {'tp_0'}, use_global_device_ids=true, to_apply=%region_7.8 | all-reduce | flops 128 | bytes 1024 | tf_op jit(solution)/shard_map/psum | solution.py:47
  100.0 15.4 %psum.57 = f32[8,16]{1,0:T(8,128)S(1)} all-reduce(f32[8,16]{1,0:T(8,128)S(1)} %psum.56), channel_id=1, replica_groups=mesh['tp_0'=8,'tp_1'=8,'dp_0'=4,'dp_1'=2] {'tp_1'}, use_global_device_ids=true, to_apply=%region_8.9 | all-reduce | flops 128 | bytes 1024 | tf_op jit(solution)/shard_map/psum | solution.py:47
  115.6 0.6 broadcast_in_dim.28
  116.2 3.3 all-to-all-start.2
  119.7 5.1 %all-to-all-done.2 = bf16[8,8,128]{2,1,0:T(8,128)(2,1)S(1)} async-done(((bf16[8,8,128]{2,1,0:T(8,128)(2,1)}), bf16[8,8,128]{2,1,0:T(8,128)(2,1)S(1)}, u32[]{:S(2)}, u32[]{:S(2)}) %all-to-all-start.2) | async-done | bytes 16416 | tf_op jit(solution)/shard_map/all_to_all | solution.py:53
  125.2 0.8 reshape.185
  126.1 8.3 %all-to-all-start.3 = ((f32[64,1,512]{2,1,0:T(1,128)}), f32[64,1,512]{2,1,0:T(1,128)S(1)}, u32[]{:S(2)}, u32[]{:S(2)}) async-start(f32[64,1,512]{2,1,0:T(1,128)} %reshape.185), calls=%async_computation.3 | async-start | bytes 262144 | tf_op jit(solution)/shard_map/all_to_all | solution.py:71
  134.5 11.7 %all-to-all-done.3 = f32[64,1,512]{2,1,0:T(1,128)S(1)} async-done(((f32[64,1,512]{2,1,0:T(1,128)}), f32[64,1,512]{2,1,0:T(1,128)S(1)}, u32[]{:S(2)}, u32[]{:S(2)}) %all-to-all-start.3) | async-done | bytes 131104 | tf_op jit(solution)/shard_map/all_to_all | solution.py:71
  146.2 0.6 broadcast.160
  146.8 1.0 reduce.11
  148.0 14.8 %psum.58 = f32[64,1]{0,1:T(1,128)S(1)} all-reduce(f32[64,1]{0,1:T(1,128)S(1)} %bitcast.277), channel_id=1, replica_groups=mesh['tp_0'=8,'tp_1'=8,'dp_0'=4,'dp_1'=2] {'tp_0'}, use_global_device_ids=true, to_apply=%region_12.13 | all-reduce | flops 64 | bytes 512 | tf_op jit(solution)/shard_map/psum | solution.py:47
  162.8 15.4 %psum.59 = f32[64,1]{0,1:T(1,128)S(1)} all-reduce(f32[64,1]{0,1:T(1,128)S(1)} %psum.58), channel_id=1, replica_groups=mesh['tp_0'=8,'tp_1'=8,'dp_0'=4,'dp_1'=2] {'tp_1'}, use_global_device_ids=true, to_apply=%region_13.14 | all-reduce | flops 64 | bytes 512 | tf_op jit(solution)/shard_map/psum | solution.py:47
  178.2 8.9 %psum.60 = f32[64,1]{0,1:T(1,128)S(1)} all-reduce(f32[64,1]{0,1:T(1,128)S(1)} %psum.59), channel_id=1, replica_groups=mesh['tp_0'=8,'tp_1'=8,'dp_0'=4,'dp_1'=2] {'dp_0'}, use_global_device_ids=true, to_apply=%region_14.15 | all-reduce | flops 64 | bytes 512 | tf_op jit(solution)/shard_map/psum | solution.py:47
  187.1 2.5 psum.61
  189.7 0.8 reshape.187
  190.4 7.7 %all-to-all-start.4 = ((bf16[64,2,256]{2,1,0:T(2,128)(2,1)}), bf16[64,2,256]{2,1,0:T(2,128)(2,1)S(1)}, u32[]{:S(2)}, u32[]{:S(2)}) async-start(bf16[64,2,256]{2,1,0:T(2,128)(2,1)} %reshape.187), calls=%async_computation.4 | async-start | bytes 131072 | tf_op jit(solution)/shard_map/all_to_all | solution.py:53
  198.3 11.2 %all-to-all-done.4 = bf16[64,2,256]{2,1,0:T(2,128)(2,1)S(1)} async-done(((bf16[64,2,256]{2,1,0:T(2,128)(2,1)}), bf16[64,2,256]{2,1,0:T(2,128)(2,1)S(1)}, u32[]{:S(2)}, u32[]{:S(2)}) %all-to-all-start.4) | async-done | bytes 65568 | tf_op jit(solution)/shard_map/all_to_all | solution.py:53
  210.8 0.7 concatenate.35
  211.5 3.4 all-to-all-start.5
  214.9 5.5 %all-to-all-done.5 = bf16[8,8,448]{2,1,0:T(8,128)(2,1)S(1)} async-done(((bf16[8,8,448]{2,1,0:T(8,128)(2,1)}), bf16[8,8,448]{2,1,0:T(8,128)(2,1)S(1)}, u32[]{:S(2)}, u32[]{:S(2)}) %all-to-all-start.5) | async-done | bytes 57376 | tf_op jit(solution)/shard_map/all_to_all | solution.py:23
  220.8 47.6 %all-gather.1 = bf16[64,32,16]{1,2,0:T(8,128)(2,1)S(1)} all-gather(bf16[1,32,16]{1,2,0:T(8,128)(2,1)S(1)} %maximum_bitcast_fusion.1), channel_id=1, replica_groups=mesh['tp_0'=8,'tp_1'=8,'dp_0'=4,'dp_1'=2] {'tp_0','tp_1'}, dimensions={0}, use_global_device_ids=true | all-gather | bytes 66560 | tf_op jit(solution)/shard_map/all_gather | solution.py:37
  268.4 0.3 reshape.170
  269.4 0.3 dynamic-slice_reduce_fusion
  269.9 0.8 fusion.1
  271.0 14.8 %psum.62 = f32[8,16]{1,0:T(8,128)S(1)} all-reduce(f32[8,16]{1,0:T(8,128)S(1)} %broadcast_multiply_fusion.2), channel_id=1, replica_groups=mesh['tp_0'=8,'tp_1'=8,'dp_0'=4,'dp_1'=2] {'tp_0'}, use_global_device_ids=true, to_apply=%region_21.22 | all-reduce | flops 128 | bytes 1024 | tf_op jit(solution)/shard_map/psum | solution.py:47
  285.8 16.7 %psum.63 = f32[8,16]{1,0:T(8,128)S(1)} all-reduce(f32[8,16]{1,0:T(8,128)S(1)} %psum.62), channel_id=1, replica_groups=mesh['tp_0'=8,'tp_1'=8,'dp_0'=4,'dp_1'=2] {'tp_1'}, use_global_device_ids=true, to_apply=%region_22.23 | all-reduce | flops 128 | bytes 1024 | tf_op jit(solution)/shard_map/psum | solution.py:47
  302.7 0.6 broadcast_in_dim.34
  303.4 3.5 %all-to-all-start.6 = ((bf16[8,8,128]{2,1,0:T(8,128)(2,1)}), bf16[8,8,128]{2,1,0:T(8,128)(2,1)S(1)}, u32[]{:S(2)}, u32[]{:S(2)}) async-start(bf16[8,8,128]{2,1,0:T(8,128)(2,1)} %broadcast_in_dim.34), calls=%async_computation.6 | async-start | bytes 32768 | tf_op jit(solution)/shard_map/all_to_all | solution.py:53
  306.9 0.6 pad_maximum_fusion.2
  307.5 0.6 pad_maximum_fusion.3
  308.1 0.6 pad_maximum_fusion.1
  308.7 3.3 all-to-all-done.6
  312.4 0.8 reshape.189
  313.2 6.4 %all-to-all-start.7 = ((f32[64,1,512]{2,1,0:T(1,128)}), f32[64,1,512]{2,1,0:T(1,128)S(1)}, u32[]{:S(2)}, u32[]{:S(2)}) async-start(f32[64,1,512]{2,1,0:T(1,128)} %reshape.189), calls=%async_computation.7 | async-start | bytes 262144 | tf_op jit(solution)/shard_map/all_to_all | solution.py:71
  319.6 0.4 multiply_add_fusion.1
  320.1 11.4 %all-to-all-done.7 = f32[64,1,512]{2,1,0:T(1,128)S(1)} async-done(((f32[64,1,512]{2,1,0:T(1,128)}), f32[64,1,512]{2,1,0:T(1,128)S(1)}, u32[]{:S(2)}, u32[]{:S(2)}) %all-to-all-start.7) | async-done | bytes 131104 | tf_op jit(solution)/shard_map/all_to_all | solution.py:71
  331.5 1.0 reduce.12
  332.7 0.8 reshape.191
  333.5 5.4 %all-to-all-start.8 = ((bf16[64,2,256]{2,1,0:T(2,128)(2,1)}), bf16[64,2,256]{2,1,0:T(2,128)(2,1)S(1)}, u32[]{:S(2)}, u32[]{:S(2)}) async-start(bf16[64,2,256]{2,1,0:T(2,128)(2,1)} %reshape.191), calls=%async_computation.8 | async-start | bytes 131072 | tf_op jit(solution)/shard_map/all_to_all | solution.py:53
  338.9 1.0 pad_maximum_fusion
  339.9 10.5 %all-to-all-done.8 = bf16[64,2,256]{2,1,0:T(2,128)(2,1)S(1)} async-done(((bf16[64,2,256]{2,1,0:T(2,128)(2,1)}), bf16[64,2,256]{2,1,0:T(2,128)(2,1)S(1)}, u32[]{:S(2)}, u32[]{:S(2)}) %all-to-all-start.8) | async-done | bytes 65568 | tf_op jit(solution)/shard_map/all_to_all | solution.py:53
  350.5 0.7 copy.102
  (129 shorter events, 7.1 us)
Async XLA Ops:
  2.3 4.4 %copy-start.14 = (f32[2,2]{1,0:T(2,128)S(1)}, f32[2,2]{1,0:T(2,128)}, u32[]{:S(2)}) copy-start(f32[2,2]{1,0:T(2,128)} %param.31) | copy-start | bytes 52
  2.3 4.5 %copy-start.10 = (f32[2,512]{1,0:T(2,128)S(1)}, f32[2,512]{1,0:T(2,128)}, u32[]{:S(2)}) copy-start(f32[2,512]{1,0:T(2,128)} %param.20) | copy-start | bytes 12292
  2.3 4.5 %copy-start.11 = (bf16[2,4,128]{2,1,0:T(4,128)(2,1)S(1)}, bf16[2,4,128]{2,1,0:T(4,128)(2,1)}, u32[]{:S(2)}) copy-start(bf16[2,4,128]{2,1,0:T(4,128)(2,1)} %param.26) | copy-start | bytes 6148
  2.3 9.6 %all-to-all-start = ((f32[8,64,1]{1,2,0:T(1,128)}), f32[8,64,1]{1,2,0:T(1,128)S(1)}, u32[]{:S(2)}, u32[]{:S(2)}) async-start(f32[8,64,1]{1,2,0:T(1,128)} %broadcast_in_dim.24), calls=%async_computation | async-start | bytes 8192 | tf_op jit(solution)/shard_map/all_to_all | solution.py:53
  6.7 1.4 copy-start.7
  6.8 0.7 copy-start.12
  7.5 0.7 copy-start.13
  8.2 0.7 copy-start.8
  8.2 0.7 copy-start.9
  8.2 0.7 copy-start.16
  8.2 0.7 copy-start.17
  8.2 0.7 copy-start.15
  8.2 3.8 %copy-start.6 = (bf16[2,512,32]{1,2,0:T(8,128)(2,1)S(1)}, bf16[2,512,32]{1,2,0:T(8,128)(2,1)}, u32[]{:S(2)}) copy-start(bf16[2,512,32]{1,2,0:T(8,128)(2,1)} %param.24) | copy-start | bytes 196612
  11.9 0.8 copy-start.5
  12.0 1.2 copy-start.3
  13.0 1.0 copy-start.2
  14.0 0.9 copy-start.4
  16.0 8.9 %all-to-all-start.1 = ((bf16[8,8,448]{2,1,0:T(8,128)(2,1)}), bf16[8,8,448]{2,1,0:T(8,128)(2,1)S(1)}, u32[]{:S(2)}, u32[]{:S(2)}) async-start(bf16[8,8,448]{2,1,0:T(8,128)(2,1)} %bitcast.6), calls=%async_computation.1 | async-start | bytes 131072 | tf_op jit(solution)/shard_map/all_to_all | solution.py:23
  81.3 1.5 copy-start
  82.8 36.8 %copy-start.1 = (bf16[2,128,512]{2,1,0:T(8,128)(2,1)S(1)}, bf16[2,128,512]{2,1,0:T(8,128)(2,1)}, u32[]{:S(2)}) copy-start(bf16[2,128,512]{2,1,0:T(8,128)(2,1)} %param.33) | copy-start | bytes 786436
  116.2 8.6 %all-to-all-start.2 = ((bf16[8,8,128]{2,1,0:T(8,128)(2,1)}), bf16[8,8,128]{2,1,0:T(8,128)(2,1)S(1)}, u32[]{:S(2)}, u32[]{:S(2)}) async-start(bf16[8,8,128]{2,1,0:T(8,128)(2,1)} %broadcast_in_dim.28), calls=%async_computation.2 | async-start | bytes 32768 | tf_op jit(solution)/shard_map/all_to_all | solution.py:53
  126.1 20.2 %all-to-all-start.3 = ((f32[64,1,512]{2,1,0:T(1,128)}), f32[64,1,512]{2,1,0:T(1,128)S(1)}, u32[]{:S(2)}, u32[]{:S(2)}) async-start(f32[64,1,512]{2,1,0:T(1,128)} %reshape.185), calls=%async_computation.3 | async-start | bytes 262144 | tf_op jit(solution)/shard_map/all_to_all | solution.py:71
  190.4 19.0 %all-to-all-start.4 = ((bf16[64,2,256]{2,1,0:T(2,128)(2,1)}), bf16[64,2,256]{2,1,0:T(2,128)(2,1)S(1)}, u32[]{:S(2)}, u32[]{:S(2)}) async-start(bf16[64,2,256]{2,1,0:T(2,128)(2,1)} %reshape.187), calls=%async_computation.4 | async-start | bytes 131072 | tf_op jit(solution)/shard_map/all_to_all | solution.py:53
  211.5 8.9 %all-to-all-start.5 = ((bf16[8,8,448]{2,1,0:T(8,128)(2,1)}), bf16[8,8,448]{2,1,0:T(8,128)(2,1)S(1)}, u32[]{:S(2)}, u32[]{:S(2)}) async-start(bf16[8,8,448]{2,1,0:T(8,128)(2,1)} %bitcast.45), calls=%async_computation.5 | async-start | bytes 131072 | tf_op jit(solution)/shard_map/all_to_all | solution.py:23
  303.4 8.6 %all-to-all-start.6 = ((bf16[8,8,128]{2,1,0:T(8,128)(2,1)}), bf16[8,8,128]{2,1,0:T(8,128)(2,1)S(1)}, u32[]{:S(2)}, u32[]{:S(2)}) async-start(bf16[8,8,128]{2,1,0:T(8,128)(2,1)} %broadcast_in_dim.34), calls=%async_computation.6 | async-start | bytes 32768 | tf_op jit(solution)/shard_map/all_to_all | solution.py:53
  313.2 18.3 %all-to-all-start.7 = ((f32[64,1,512]{2,1,0:T(1,128)}), f32[64,1,512]{2,1,0:T(1,128)S(1)}, u32[]{:S(2)}, u32[]{:S(2)}) async-start(f32[64,1,512]{2,1,0:T(1,128)} %reshape.189), calls=%async_computation.7 | async-start | bytes 262144 | tf_op jit(solution)/shard_map/all_to_all | solution.py:71
  333.5 16.9 %all-to-all-start.8 = ((bf16[64,2,256]{2,1,0:T(2,128)(2,1)}), bf16[64,2,256]{2,1,0:T(2,128)(2,1)S(1)}, u32[]{:S(2)}, u32[]{:S(2)}) async-start(bf16[64,2,256]{2,1,0:T(2,128)(2,1)} %reshape.191), calls=%async_computation.8 | async-start | bytes 131072 | tf_op jit(solution)/shard_map/all_to_all | solution.py:53
where the time goes:
time: 352 us; the launch traced here: 351 us
  blocking collectives  208 us (59%)
  waiting for transfers between devices  67.3 us (19%)
  starting transfers between devices  45.8 us (13%)
  local copies, waits for them, and re-layouts  16.8 us (5%)
  other arithmetic  7.6 us (2%)
  matrix products  4.45 us (1%)
    psum x8, blocking collectives, over_axes(): shard = lax.psum(shard, axis)  104 us
    all_gather x2, blocking collectives, gather_turned(): lax.all_gather(both, axis, axis=0, tiled=True)  104 us
    all_to_all x5, waiting for transfers between devices, copy_for_each(): lax.all_to_all(jnp.broadcast_to(shard[None], (size, *shard.shape)), axis,...  33 us
    all_to_all x5, starting transfers between devices, copy_for_each(): lax.all_to_all(jnp.broadcast_to(shard[None], (size, *shard.shape)), axis,...  24.4 us
    all_to_all x2, waiting for transfers between devices, summed_on_arrival_2(): lax.all_to_all(pieces, axis, split_axis=0, concat_axis=0, tiled=True)  23.2 us
    all_to_all x2, starting transfers between devices, summed_on_arrival_2(): lax.all_to_all(pieces, axis, split_axis=0, concat_axis=0, tiled=True)  14.7 us
    all_to_all x2, waiting for transfers between devices, summed_on_arrival(): pieces = lax.all_to_all(cut_along(shard, dim, size), axis, 0, 0, tiled=True)  11.1 us
    unnamed x52, local copies, waits for them, and re-layouts  9.87 us
  transfers between devices with their start and end apart: 9, of which 9 were waited for; matrix products, arithmetic and copies ran while one was open for 1% of the time, Pallas kernels for 0%

commit v1 on v0

--- a/solution.py
+++ b/solution.py
@@ -44,7 +44,7 @@
 
 def over_axes(shard, axes):
     for axis in axes:
-        shard = lax.psum(shard, axis)
+        shard = jnp.sum(lax.all_gather(shard, axis), axis=0)
     return shard
 
 

time: 352 us -> 390 us (1.11)
  blocking collectives: 208 us -> 244 us
  waiting for transfers between devices: 67.3 us -> 59.8 us
  local copies, waits for them, and re-layouts: 16.8 us -> 23.1 us
    psum x8 -> x0, blocking collectives: 104 us -> none  [over_axes(): shard = lax.psum(shard, axis)]
    all_gather x0 -> x4, blocking collectives: none -> 98.5 us  [over_axes(): shard = jnp.sum(lax.all_gather(shard, axis), axis=0)]
    unnamed x0 -> x4, blocking collectives: none -> 41.5 us
    all_to_all x2, waiting for transfers between devices: 23.2 us -> 15.5 us  [summed_on_arrival_2(): lax.all_to_all(pieces, axis, split_axis=0, concat_axis=0, tiled=True)]
    unnamed x52 -> x64, local copies, waits for them, and re-layouts: 9.87 us -> 15.9 us
  transfers between devices with their start and end apart: 9 -> 9, of which waited for: 9 -> 9; matrix products, arithmetic and copies ran while one was open for 1% -> 2% of each run, Pallas kernels for 0% -> 0%
where the time goes in v1:
time: 390 us; the launch traced here: 389 us
  blocking collectives  244 us (63%)
  waiting for transfers between devices  59.8 us (15%)
  starting transfers between devices  45.8 us (12%)
  local copies, waits for them, and re-layouts  23.1 us (6%)
  other arithmetic  7.74 us (2%)
  matrix products  4.45 us (1%)
  between operations  3.9 us (1%)
    all_gather x2, blocking collectives, gather_turned(): lax.all_gather(both, axis, axis=0, tiled=True)  104 us
    all_gather x4, blocking collectives, over_axes(): shard = jnp.sum(lax.all_gather(shard, axis), axis=0)  98.5 us
    unnamed x4, blocking collectives  41.5 us
    all_to_all x5, waiting for transfers between devices, copy_for_each(): lax.all_to_all(jnp.broadcast_to(shard[None], (size, *shard.shape)), axis,...  33.3 us
    all_to_all x5, starting transfers between devices, copy_for_each(): lax.all_to_all(jnp.broadcast_to(shard[None], (size, *shard.shape)), axis,...  24.4 us
    unnamed x64, local copies, waits for them, and re-layouts  15.9 us
    all_to_all x2, waiting for transfers between devices, summed_on_arrival_2(): lax.all_to_all(pieces, axis, split_axis=0, concat_axis=0, tiled=True)  15.5 us
    all_to_all x2, starting transfers between devices, summed_on_arrival_2(): lax.all_to_all(pieces, axis, split_axis=0, concat_axis=0, tiled=True)  14.7 us
  transfers between devices with their start and end apart: 9, of which 9 were waited for; matrix products, arithmetic and copies ran while one was open for 2% of the time, Pallas kernels for 0%

profile of v1, /device:TPU:8, one launch (start us, length us, event | category | flops | bytes accessed | tf_op | source)
XLA Modules:
  0.0 388.6 jit_solution(14166485167418932632)
XLA Ops:
  0.6 1.0 copy.87
  1.7 0.6 broadcast_in_dim.22
  2.3 4.4 %all-to-all-start = ((f32[8,64,1]{1,2,0:T(1,128)}), f32[8,64,1]{1,2,0:T(1,128)S(1)}, u32[]{:S(2)}, u32[]{:S(2)}) async-start(f32[8,64,1]{1,2,0:T(1,128)} %broadcast_in_dim.22), calls=%async_computation | async-start | bytes 8192 | tf_op jit(solution)/shard_map/all_to_all | solution.py:53
  6.8 0.6 copy-done.10
  7.5 0.7 copy-done.13
  8.2 0.7 copy-done.8
  8.9 3.0 all-to-all-done
  12.3 0.4 copy-done.5
  13.2 0.3 convolution_convert_fusion.4
  13.5 0.5 copy-done.2
  14.0 0.3 convolution_convert_fusion.3
  14.3 0.6 copy-done.4
  14.9 0.3 convolution_convert_fusion.5
  15.3 0.7 concatenate.30
  16.0 3.4 all-to-all-start.1
  19.4 5.5 %all-to-all-done.1 = bf16[8,8,448]{2,1,0:T(8,128)(2,1)S(1)} async-done(((bf16[8,8,448]{2,1,0:T(8,128)(2,1)}), bf16[8,8,448]{2,1,0:T(8,128)(2,1)S(1)}, u32[]{:S(2)}, u32[]{:S(2)}) %all-to-all-start.1) | async-done | bytes 57376 | tf_op jit(solution)/shard_map/all_to_all | solution.py:23
  25.2 56.1 %all-gather.6 = bf16[64,32,16]{1,2,0:T(8,128)(2,1)S(1)} all-gather(bf16[1,32,16]{1,2,0:T(8,128)(2,1)S(1)} %maximum_bitcast_fusion), channel_id=1, replica_groups=mesh['tp_0'=8,'tp_1'=8,'dp_0'=4,'dp_1'=2] {'tp_0','tp_1'}, dimensions={0}, use_global_device_ids=true | all-gather | bytes 66560 | tf_op jit(solution)/shard_map/all_gather | solution.py:37
  81.4 0.3 reshape.287
  82.8 0.8 fusion.4
  84.0 24.7 %all_gather.48 = f32[8,8,16]{2,1,0:T(8,128)S(1)} all-gather(f32[1,8,16]{2,1,0:T(8,128)S(1)} %broadcast_multiply_fusion.3), channel_id=1, replica_groups=mesh['tp_0'=8,'tp_1'=8,'dp_0'=4,'dp_1'=2] {'tp_0'}, dimensions={0}, use_global_device_ids=true | all-gather | bytes 4608 | tf_op jit(solution)/shard_map/all_gather | solution.py:47
  108.7 24.5 %all-gather = f32[64,16]{1,0:T(8,128)S(1)} all-gather(f32[8,16]{1,0:T(8,128)S(1)} %reduce_sum.247), channel_id=2, replica_groups=mesh['tp_0'=8,'tp_1'=8,'dp_0'=4,'dp_1'=2] {'tp_1'}, dimensions={0}, use_global_device_ids=true | all-gather | bytes 4608 | tf_op jit(solution)/shard_map/all_gather | solution.py:47
  133.4 0.6 broadcast_in_dim.26
  134.0 3.3 all-to-all-start.2
  137.5 5.1 %all-to-all-done.2 = bf16[8,8,128]{2,1,0:T(8,128)(2,1)S(1)} async-done(((bf16[8,8,128]{2,1,0:T(8,128)(2,1)}), bf16[8,8,128]{2,1,0:T(8,128)(2,1)S(1)}, u32[]{:S(2)}, u32[]{:S(2)}) %all-to-all-start.2) | async-done | bytes 16416 | tf_op jit(solution)/shard_map/all_to_all | solution.py:53
  143.1 0.8 reshape.312
  143.9 8.3 %all-to-all-start.3 = ((f32[64,1,512]{2,1,0:T(1,128)}), f32[64,1,512]{2,1,0:T(1,128)S(1)}, u32[]{:S(2)}, u32[]{:S(2)}) async-start(f32[64,1,512]{2,1,0:T(1,128)} %reshape.312), calls=%async_computation.3 | async-start | bytes 262144 | tf_op jit(solution)/shard_map/all_to_all | solution.py:71
  152.3 1.3 dynamic-slice.4
  153.5 1.3 dynamic-slice.3
  156.1 1.3 dynamic-slice.2
  158.0 1.3 dynamic-slice.1
  160.0 4.0 %all-to-all-done.3 = f32[64,1,512]{2,1,0:T(1,128)S(1)} async-done(((f32[64,1,512]{2,1,0:T(1,128)}), f32[64,1,512]{2,1,0:T(1,128)S(1)}, u32[]{:S(2)}, u32[]{:S(2)}) %all-to-all-start.3) | async-done | bytes 131104 | tf_op jit(solution)/shard_map/all_to_all | solution.py:71
  164.1 0.6 broadcast.240
  164.7 1.0 reduce.19
  166.1 14.7 %all-reduce = f32[512]{0:T(512)S(1)} all-reduce(f32[512]{0:T(512)S(1)} %dynamic-update-slice), channel_id=3, replica_groups=mesh['tp_0'=8,'tp_1'=8,'dp_0'=4,'dp_1'=2] {'tp_0'}, use_global_device_ids=true, to_apply=%add | all-reduce | flops 512 | bytes 4096
  181.2 15.4 %all-reduce.1 = f32[512]{0:T(512)S(1)} all-reduce(f32[512]{0:T(512)S(1)} %dynamic-update-slice.1), channel_id=4, replica_groups=mesh['tp_0'=8,'tp_1'=8,'dp_0'=4,'dp_1'=2] {'tp_1'}, use_global_device_ids=true, to_apply=%add.1 | all-reduce | flops 512 | bytes 4096
  197.0 8.9 %all-reduce.2 = f32[256]{0:T(256)S(1)} all-reduce(f32[256]{0:T(256)S(1)} %dynamic-update-slice.2), channel_id=5, replica_groups=mesh['tp_0'=8,'tp_1'=8,'dp_0'=4,'dp_1'=2] {'dp_0'}, use_global_device_ids=true, to_apply=%add.2 | all-reduce | flops 256 | bytes 2048
  206.2 2.4 all-reduce.3
  208.9 0.8 reshape.314
  209.6 7.9 %all-to-all-start.4 = ((bf16[64,2,256]{2,1,0:T(2,128)(2,1)}), bf16[64,2,256]{2,1,0:T(2,128)(2,1)S(1)}, u32[]{:S(2)}, u32[]{:S(2)}) async-start(bf16[64,2,256]{2,1,0:T(2,128)(2,1)} %reshape.314), calls=%async_computation.4 | async-start | bytes 131072 | tf_op jit(solution)/shard_map/all_to_all | solution.py:53
  217.7 11.2 %all-to-all-done.4 = bf16[64,2,256]{2,1,0:T(2,128)(2,1)S(1)} async-done(((bf16[64,2,256]{2,1,0:T(2,128)(2,1)}), bf16[64,2,256]{2,1,0:T(2,128)(2,1)S(1)}, u32[]{:S(2)}, u32[]{:S(2)}) %all-to-all-start.4) | async-done | bytes 65568 | tf_op jit(solution)/shard_map/all_to_all | solution.py:53
  230.2 0.7 concatenate.35
  230.9 3.4 all-to-all-start.5
  234.3 5.5 %all-to-all-done.5 = bf16[8,8,448]{2,1,0:T(8,128)(2,1)S(1)} async-done(((bf16[8,8,448]{2,1,0:T(8,128)(2,1)}), bf16[8,8,448]{2,1,0:T(8,128)(2,1)S(1)}, u32[]{:S(2)}, u32[]{:S(2)}) %all-to-all-start.5) | async-done | bytes 57376 | tf_op jit(solution)/shard_map/all_to_all | solution.py:23
  240.2 47.8 %all-gather.7 = bf16[64,32,16]{1,2,0:T(8,128)(2,1)S(1)} all-gather(bf16[1,32,16]{1,2,0:T(8,128)(2,1)S(1)} %maximum_bitcast_fusion.1), channel_id=1, replica_groups=mesh['tp_0'=8,'tp_1'=8,'dp_0'=4,'dp_1'=2] {'tp_0','tp_1'}, dimensions={0}, use_global_device_ids=true | all-gather | bytes 66560 | tf_op jit(solution)/shard_map/all_gather | solution.py:37
  288.0 0.3 reshape.289
  289.5 0.8 fusion.1
  290.6 24.7 %all_gather.59 = f32[8,8,16]{2,1,0:T(8,128)S(1)} all-gather(f32[1,8,16]{2,1,0:T(8,128)S(1)} %broadcast_multiply_fusion.2), channel_id=1, replica_groups=mesh['tp_0'=8,'tp_1'=8,'dp_0'=4,'dp_1'=2] {'tp_0'}, dimensions={0}, use_global_device_ids=true | all-gather | bytes 4608 | tf_op jit(solution)/shard_map/all_gather | solution.py:47
  315.3 24.7 %all-gather.5 = f32[64,16]{1,0:T(8,128)S(1)} all-gather(f32[8,16]{1,0:T(8,128)S(1)} %reduce_sum.264), channel_id=7, replica_groups=mesh['tp_0'=8,'tp_1'=8,'dp_0'=4,'dp_1'=2] {'tp_1'}, dimensions={0}, use_global_device_ids=true | all-gather | bytes 4608 | tf_op jit(solution)/shard_map/all_gather | solution.py:47
  340.2 0.6 broadcast_in_dim.31
  340.8 3.3 all-to-all-start.6
  344.1 0.6 pad_maximum_fusion.2
  344.8 0.6 pad_maximum_fusion.3
  345.4 0.6 pad_maximum_fusion.1
  346.0 3.5 all-to-all-done.6
  349.8 0.8 reshape.316
  350.7 6.4 %all-to-all-start.7 = ((f32[64,1,512]{2,1,0:T(1,128)}), f32[64,1,512]{2,1,0:T(1,128)S(1)}, u32[]{:S(2)}, u32[]{:S(2)}) async-start(f32[64,1,512]{2,1,0:T(1,128)} %reshape.316), calls=%async_computation.7 | async-start | bytes 262144 | tf_op jit(solution)/shard_map/all_to_all | solution.py:71
  357.0 0.4 multiply_add_fusion.1
  357.4 11.4 %all-to-all-done.7 = f32[64,1,512]{2,1,0:T(1,128)S(1)} async-done(((f32[64,1,512]{2,1,0:T(1,128)}), f32[64,1,512]{2,1,0:T(1,128)S(1)}, u32[]{:S(2)}, u32[]{:S(2)}) %all-to-all-start.7) | async-done | bytes 131104 | tf_op jit(solution)/shard_map/all_to_all | solution.py:71
  368.9 1.0 reduce.20
  370.1 0.8 reshape.318
  370.9 5.4 %all-to-all-start.8 = ((bf16[64,2,256]{2,1,0:T(2,128)(2,1)}), bf16[64,2,256]{2,1,0:T(2,128)(2,1)S(1)}, u32[]{:S(2)}, u32[]{:S(2)}) async-start(bf16[64,2,256]{2,1,0:T(2,128)(2,1)} %reshape.318), calls=%async_computation.8 | async-start | bytes 131072 | tf_op jit(solution)/shard_map/all_to_all | solution.py:53
  376.2 1.0 pad_maximum_fusion
  377.3 10.5 %all-to-all-done.8 = bf16[64,2,256]{2,1,0:T(2,128)(2,1)S(1)} async-done(((bf16[64,2,256]{2,1,0:T(2,128)(2,1)}), bf16[64,2,256]{2,1,0:T(2,128)(2,1)S(1)}, u32[]{:S(2)}, u32[]{:S(2)}) %all-to-all-start.8) | async-done | bytes 65568 | tf_op jit(solution)/shard_map/all_to_all | solution.py:53
  387.9 0.7 copy.102
  (153 shorter events, 9.5 us)
Async XLA Ops:
  2.3 4.4 %copy-start.14 = (f32[2,2]{1,0:T(2,128)S(1)}, f32[2,2]{1,0:T(2,128)}, u32[]{:S(2)}) copy-start(f32[2,2]{1,0:T(2,128)} %param.31) | copy-start | bytes 52
  2.3 4.5 %copy-start.15 = (f32[2,128]{1,0:T(2,128)S(1)}, f32[2,128]{1,0:T(2,128)}, u32[]{:S(2)}) copy-start(f32[2,128]{1,0:T(2,128)} %param.32) | copy-start | bytes 3076
  2.3 9.6 %all-to-all-start = ((f32[8,64,1]{1,2,0:T(1,128)}), f32[8,64,1]{1,2,0:T(1,128)S(1)}, u32[]{:S(2)}, u32[]{:S(2)}) async-start(f32[8,64,1]{1,2,0:T(1,128)} %broadcast_in_dim.22), calls=%async_computation | async-start | bytes 8192 | tf_op jit(solution)/shard_map/all_to_all | solution.py:53
  6.7 0.7 copy-start.10
  6.7 0.7 copy-start.11
  6.7 0.7 copy-start.12
  7.4 0.7 copy-start.7
  7.4 0.7 copy-start.13
  8.1 0.7 copy-start.8
  8.1 0.7 copy-start.9
  8.1 0.7 copy-start.16
  8.1 0.7 copy-start.17
  8.2 3.8 copy-start.6
  11.9 0.8 copy-start.5
  12.0 1.2 copy-start.3
  13.0 1.0 copy-start.2
  14.0 0.9 copy-start.4
  16.0 8.9 %all-to-all-start.1 = ((bf16[8,8,448]{2,1,0:T(8,128)(2,1)}), bf16[8,8,448]{2,1,0:T(8,128)(2,1)S(1)}, u32[]{:S(2)}, u32[]{:S(2)}) async-start(bf16[8,8,448]{2,1,0:T(8,128)(2,1)} %bitcast.6), calls=%async_computation.1 | async-start | bytes 131072 | tf_op jit(solution)/shard_map/all_to_all | solution.py:23
  81.3 1.5 copy-start
  83.6 53.7 %copy-start.1 = (bf16[2,128,512]{2,1,0:T(8,128)(2,1)S(1)}, bf16[2,128,512]{2,1,0:T(8,128)(2,1)}, u32[]{:S(2)}) copy-start(bf16[2,128,512]{2,1,0:T(8,128)(2,1)} %param.33) | copy-start | bytes 786436
  134.0 8.6 %all-to-all-start.2 = ((bf16[8,8,128]{2,1,0:T(8,128)(2,1)}), bf16[8,8,128]{2,1,0:T(8,128)(2,1)S(1)}, u32[]{:S(2)}, u32[]{:S(2)}) async-start(bf16[8,8,128]{2,1,0:T(8,128)(2,1)} %broadcast_in_dim.26), calls=%async_computation.2 | async-start | bytes 32768 | tf_op jit(solution)/shard_map/all_to_all | solution.py:53
  143.9 20.2 %all-to-all-start.3 = ((f32[64,1,512]{2,1,0:T(1,128)}), f32[64,1,512]{2,1,0:T(1,128)S(1)}, u32[]{:S(2)}, u32[]{:S(2)}) async-start(f32[64,1,512]{2,1,0:T(1,128)} %reshape.312), calls=%async_computation.3 | async-start | bytes 262144 | tf_op jit(solution)/shard_map/all_to_all | solution.py:71
  209.6 19.2 %all-to-all-start.4 = ((bf16[64,2,256]{2,1,0:T(2,128)(2,1)}), bf16[64,2,256]{2,1,0:T(2,128)(2,1)S(1)}, u32[]{:S(2)}, u32[]{:S(2)}) async-start(bf16[64,2,256]{2,1,0:T(2,128)(2,1)} %reshape.314), calls=%async_computation.4 | async-start | bytes 131072 | tf_op jit(solution)/shard_map/all_to_all | solution.py:53
  230.9 8.9 %all-to-all-start.5 = ((bf16[8,8,448]{2,1,0:T(8,128)(2,1)}), bf16[8,8,448]{2,1,0:T(8,128)(2,1)S(1)}, u32[]{:S(2)}, u32[]{:S(2)}) async-start(bf16[8,8,448]{2,1,0:T(8,128)(2,1)} %bitcast.48), calls=%async_computation.5 | async-start | bytes 131072 | tf_op jit(solution)/shard_map/all_to_all | solution.py:23
  340.8 8.6 %all-to-all-start.6 = ((bf16[8,8,128]{2,1,0:T(8,128)(2,1)}), bf16[8,8,128]{2,1,0:T(8,128)(2,1)S(1)}, u32[]{:S(2)}, u32[]{:S(2)}) async-start(bf16[8,8,128]{2,1,0:T(8,128)(2,1)} %broadcast_in_dim.31), calls=%async_computation.6 | async-start | bytes 32768 | tf_op jit(solution)/shard_map/all_to_all | solution.py:53
  350.7 18.2 %all-to-all-start.7 = ((f32[64,1,512]{2,1,0:T(1,128)}), f32[64,1,512]{2,1,0:T(1,128)S(1)}, u32[]{:S(2)}, u32[]{:S(2)}) async-start(f32[64,1,512]{2,1,0:T(1,128)} %reshape.316), calls=%async_computation.7 | async-start | bytes 262144 | tf_op jit(solution)/shard_map/all_to_all | solution.py:71
  370.9 16.9 %all-to-all-start.8 = ((bf16[64,2,256]{2,1,0:T(2,128)(2,1)}), bf16[64,2,256]{2,1,0:T(2,128)(2,1)S(1)}, u32[]{:S(2)}, u32[]{:S(2)}) async-start(bf16[64,2,256]{2,1,0:T(2,128)(2,1)} %reshape.318), calls=%async_computation.8 | async-start | bytes 131072 | tf_op jit(solution)/shard_map/all_to_all | solution.py:53
